TPU v7x, 32 devices: a whole 2x2x4 slice. The times are simulated.
32 devices in a mesh: grp: 2 (over y), sp: 4 (over z), tp: 4 (over x, core).
Axes of the slice: x: 2, y: 2, z: 4, core: 2. Of those that a mesh axis runs over, the one named last changes fastest.
Arguments:
- layer_feed: bfloat16 [4, 2048, 4096], P('grp', 'sp'), parts along dimension 0, may hold values from -13 to 13
- address_mapping: bfloat16 [4096, 2048], P(None, 'tp'), may hold values from -0.09375 to 0.09375
- content_mapping: bfloat16 [4096, 2048], P(None, 'tp'), may hold values from -0.09375 to 0.09375
- beta_mapping_matrix: bfloat16 [4096, 32], replicated, may hold values from -0.032958984 to 0.029541016
- forgetting_mapping: bfloat16 [4096, 32], replicated, may hold values from -0.09375 to 0.09375
- logged_fading_speed: float32 [32], P('tp'), may hold values from -12 to -2.8
- extra_forgetting: bfloat16 [4, 2048, 32], P('grp', 'sp', 'tp'), parts along dimension 0, may hold values from -1.4 to 0
- opening_probe: bfloat16 [4, 2048], P('grp', 'tp'), parts along dimension 0, may hold values from -6 to 6
Outputs:
- context_memory_tensor: bfloat16 [4, 32, 64, 64], P('grp', 'tp', 'sp'), parts along dimension 0
- opening_normed_output: bfloat16 [4, 2048], P('grp', 'tp'), parts along dimension 0
There are 2 independent parts, one for each index of `grp`. A program takes and returns all parts, laid end to end along the dimension named above; an argument that names none is the same for every part. Nothing has to cross between parts.
All inputs are finite; a program needn't handle non-finite values.
Results may differ from a plain program's by a relative error of at most 0.014.
Values sent between devices are 32-bit elements; how exact they have to be, the bound alone decides.
A program may use at most 64 MiB of HBM per device.

v0:
```python
import math

import jax
import jax.numpy as jnp
from jax import lax
from jax.sharding import PartitionSpec as P

HEAD = 64


finest = lax.Precision.HIGHEST


def prefix(part, axis, combine, identity):
    count = lax.axis_size(axis)
    place = lax.axis_index(axis)
    ahead = count - 1 - place
    gathered = lax.all_gather(part, axis)
    state = jnp.zeros_like(part) + jnp.asarray(identity, part.dtype)

    def one(hop, state):
        source = count - 1 - hop
        return combine(state, lax.dynamic_index_in_dim(gathered, source, 0, False))

    return lax.fori_loop(0, ahead, one, state)


def head_columns(weight, heads):
    first = lax.axis_index("tp") * heads
    return lax.dynamic_slice_in_dim(weight, first, heads, 1)


def compute_states(
    address_embeddings,
    content_embeddings,
    beta_raw_scores,
    forgetting_raw_scores,
    extra_forgetting,
    logged_fading_speed,
):
    seqs, length, width = address_embeddings.shape
    heads = width // HEAD
    keys = jax.nn.silu(address_embeddings.astype(jnp.float32)).reshape(seqs, length, heads, HEAD)
    keys = keys * lax.rsqrt(jnp.sum(keys * keys, axis=-1, keepdims=True) + 1e-06)
    values = jax.nn.silu(content_embeddings.astype(jnp.float32)).reshape(seqs, length, heads, HEAD)
    betas = jax.nn.sigmoid(beta_raw_scores.astype(jnp.float32))
    decay_factors = -jnp.exp(logged_fading_speed) * jax.nn.softplus(
        forgetting_raw_scores.astype(jnp.float32)
    ) + extra_forgetting.astype(jnp.float32)
    groups = seqs * heads
    keys = keys.transpose(0, 2, 1, 3).reshape(groups, length, HEAD)
    values = values.transpose(0, 2, 1, 3).reshape(groups, length, HEAD)
    betas = betas.transpose(0, 2, 1).reshape(groups, length)
    decay_factors = decay_factors.transpose(0, 2, 1).reshape(groups, length)
    return (keys, values, betas, decay_factors)


def block_parts(keys, values, betas, decay_factors):
    groups, length, width = keys.shape
    size = math.gcd(length, 64)
    count = length // size
    keys = keys.reshape(groups, count, size, width)
    values = values.reshape(groups, count, size, width)
    betas = betas.reshape(groups, count, size)
    cumul = jnp.cumsum(decay_factors.reshape(groups, count, size), axis=-1)
    rows_idx = lax.broadcasted_iota(jnp.int32, (size, size), 0)
    cols_idx = lax.broadcasted_iota(jnp.int32, (size, size), 1)
    below = rows_idx > cols_idx
    spread = jnp.where(below, cumul[..., :, None] - cumul[..., None, :], 0.0)
    weights = jnp.where(below, jnp.exp(spread), 0.0)
    gram = jnp.einsum("gnid,gnjd->gnij", keys, keys, precision=finest)
    lower = jnp.eye(size, dtype=jnp.float32) + betas[..., :, None] * gram * weights
    right = jnp.concatenate(
        [values * betas[..., None], keys * (betas * jnp.exp(cumul))[..., None]], axis=-1
    )
    solved = jax.scipy.linalg.solve_triangular(lower, right, lower=True)
    update = solved[..., :width]
    mixing = solved[..., width:]
    carried = keys * jnp.exp(cumul[..., -1:] - cumul)[..., None]
    closing = jnp.exp(cumul[..., -1])
    return (update, mixing, carried, closing)


def run_blocks(start, parts, padding):

    def advance(state, piece):
        update, mixing, carried, closing = piece
        update = jnp.concatenate(
            [jnp.zeros(update.shape[:-1] + (padding,), jnp.float32), update], axis=-1
        )
        fresh = update - jnp.einsum("gck,gkw->gcw", mixing, state, precision=finest)
        state = closing[:, None, None] * state + jnp.einsum(
            "gck,gcw->gkw", carried, fresh, precision=finest
        )
        return (state, None)

    moved = tuple((jnp.moveaxis(member, 1, 0) for member in parts))
    final, _ = lax.scan(advance, start, moved)
    return final


def matmul(left, right):
    return jnp.einsum("shij,shjk->shik", left, right, precision=finest)


def body(
    layer_feed,
    address_mapping,
    content_mapping,
    beta_mapping_matrix,
    forgetting_mapping,
    logged_fading_speed,
    extra_forgetting,
    opening_probe,
):
    heads = address_mapping.shape[1] // HEAD
    seqs_all = layer_feed.shape[0]
    address_embeddings = jnp.dot(
        layer_feed, address_mapping, preferred_element_type=jnp.float32
    ).astype(jnp.bfloat16)
    content_embeddings = jnp.dot(
        layer_feed, content_mapping, preferred_element_type=jnp.float32
    ).astype(jnp.bfloat16)
    beta_raw_scores = jnp.dot(
        layer_feed, head_columns(beta_mapping_matrix, heads), preferred_element_type=jnp.float32
    ).astype(jnp.bfloat16)
    forgetting_raw_scores = jnp.dot(
        layer_feed, head_columns(forgetting_mapping, heads), preferred_element_type=jnp.float32
    ).astype(jnp.bfloat16)
    keys, values, betas, decay_factors = compute_states(
        address_embeddings,
        content_embeddings,
        beta_raw_scores,
        forgetting_raw_scores,
        extra_forgetting,
        logged_fading_speed,
    )
    parts = block_parts(keys, values, betas, decay_factors)
    opening = jnp.concatenate(
        [jnp.eye(HEAD, dtype=jnp.float32), jnp.zeros((HEAD, HEAD), jnp.float32)], axis=1
    )
    start = jnp.broadcast_to(opening, (seqs_all * heads, HEAD, 2 * HEAD))
    joined = run_blocks(start, parts, HEAD).reshape(seqs_all, heads, HEAD, 2 * HEAD)
    transfer = joined[..., :HEAD]
    offset = joined[..., HEAD:]
    identity = jnp.broadcast_to(jnp.eye(HEAD, dtype=jnp.float32), transfer.shape)
    rows = HEAD // lax.axis_size("sp")
    first_row = lax.axis_index("sp") * rows
    suffix = prefix(transfer, "sp", matmul, identity)
    terms = matmul(suffix, offset)
    final = lax.psum_scatter(terms, "sp", scatter_dimension=2, tiled=True)
    context_memory_tensor = final.astype(jnp.bfloat16)
    query_per_head = opening_probe.reshape(seqs_all, heads, HEAD)
    query_rows = lax.dynamic_slice_in_dim(query_per_head, first_row, rows, 2).astype(jnp.float32)
    partial_read = jnp.einsum("shk,shkv->shv", query_rows, final, precision=finest)
    state_readout = lax.psum(partial_read, "sp")
    state_readout = state_readout * lax.rsqrt(
        jnp.mean(state_readout * state_readout, axis=-1, keepdims=True) + 1e-06
    )
    opening_normed_output = state_readout.reshape(seqs_all, heads * HEAD).astype(jnp.bfloat16)
    return (context_memory_tensor, opening_normed_output)


def solution(mesh):
    in_specs = (
        P("grp", "sp", None),
        P(None, "tp"),
        P(None, "tp"),
        P(),
        P(),
        P("tp"),
        P("grp", "sp", "tp"),
        P("grp", "tp"),
    )
    out_specs = (P("grp", "tp", "sp", None), P("grp", "tp"))
    return jax.shard_map(body, mesh=mesh, in_specs=in_specs, out_specs=out_specs, check_vma=False)
```

profile of v0, /device:TPU:0, one launch (start us, length us, event | category | flops | bytes accessed | tf_op | source)
XLA Modules:
  0.0 849.0 jit_solution(2494911907279532112)
XLA Ops:
  8.1 5.7 fusion.51
  13.9 3.5 reduce_window_sum.11
  17.7 5.7 fusion.40
  23.5 8.7 %multiply_reduce_fusion = (f32[2,512,8]{1,2,0:T(8,128)S(1)}, f32[2,512,512]{1,2,0:T(8,128)S(1)}) fusion(bf16[2,512,4096]{2,1,0:T(8,128)(2,1)} %param.12, bf16[4096,512]{1,0:T(8,128)(2,1)} %param.13), kind=kOutput, calls=%fused_computation.41 | convolution fusion | flops 4299153408 | bytes 14712832 | tf_op jit(solution)/shard_map/dot_general | solution.py:118
  32.2 2.7 copy.28
  35.1 3.7 broadcast_multiply_fusion.2
  38.8 1.9 copy-done.4
  40.7 8.8 %select_bitcast_fusion = f32[16,8,1,64,64]{4,3,2,1,0:T(8,128)} fusion(f32[16,8,64,64]{3,2,1,0:T(8,128)S(1)} %bitcast.118, f32[16,8,64]{2,1,0:T(8,128)S(1)} %reduce_window_sum.11, f32[16,8,64]{2,1,0:T(8,128)S(1)} %mul.105, f32[64,64]{1,0:T(8,128)S(1)} %fusion.54, pred[64,64]{1,0:T(8,128)(4,1)S(1)} %get-tuple-element.140, ...), kind=kOutput, calls=%fused_computation.26 | convolution fusion | flops 406323200 | bytes 4284416 | tf_op jit(solution)/shard_map/gnid,gnjd->gnij/dot_general | solution.py:71
  49.5 630.6 %custom-call.4 = f32[16,8,1,64,64]{3,4,2,1,0:T(8,128)} custom-call(f32[16,8,1,64,64]{4,3,2,1,0:T(8,128)} %select_bitcast_fusion), custom_call_target="InvertDiagBlocksLowerTriangular" | custom-call | tf_op jit(solution)/shard_map/jit(_solve_triangular)/vmap(vmap())/triangular_solve | solution.py:76
  680.0 8.7 %convert_multiply_fusion = f32[2,512,512]{1,2,0:T(8,128)S(1)} fusion(bf16[2,512,4096]{2,1,0:T(8,128)(2,1)} %param.12, bf16[4096,512]{1,0:T(8,128)(2,1)} %param.14), kind=kOutput, calls=%fused_computation.28 | convolution fusion | flops 4298113024 | bytes 14680064 | tf_op jit(solution)/shard_map/dot_general | solution.py:121
  688.7 2.7 copy.31
  691.5 3.0 broadcast_multiply_fusion.1
  694.9 3.8 broadcast_multiply_fusion
  698.7 7.9 fusion.10
  706.6 4.9 slice_bitcast_fusion
  711.6 40.2 %while.22 = (s32[]{:T(128)}, f32[16,64,128]{2,1,0:T(8,128)S(1)}, f32[8,16]{1,0:T(8,128)S(1)}, f32[8,16,64,64]{3,2,0,1:T(8,128)}, f32[8,16,64,64]{3,2,0,1:T(8,128)}, /*index=5*/f32[8,16,64,64]{3,2,0,1:T(8,128)}, s32[]{:T(128)}) while((s32[]{:T(128)}, f32[16,64,128]{2,1,0:T(8,128)S(1)}, f32[8,16]{1,0:T(8,128)S(1)}, f32[8,16,64,64]{3,2,0,1:T(8,128)}, ...), condition=%wide.region_3.4_spmd, body=%wide.region_2.3_spmd.sunk | while | flops 201719808 | bytes 4457749 | solution.py:98
  714.5 2.2 convolution_add_fusion.2
  719.5 2.2 convolution_add_fusion.2
  724.5 2.2 convolution_add_fusion.2
  729.5 2.2 convolution_add_fusion.2
  734.6 2.2 convolution_add_fusion.2
  739.6 2.2 convolution_add_fusion.2
  744.6 2.2 convolution_add_fusion.2
  749.6 2.2 convolution_add_fusion.2
  752.8 48.4 %all-gather.3.cloned.1.call-done = f32[8,8,64,64]{3,2,1,0:T(8,128)} async-done(((f32[2,8,64,64]{3,2,1,0:T(8,128)}), f32[8,8,64,64]{3,2,1,0:T(8,128)}) %all-gather.3.cloned.1.call-update) | async-done | bytes 1048592 | tf_op jit(solution)/shard_map/all_gather | solution.py:18
  801.2 6.5 while.23
  801.3 2.1 convolution_bitcast_fusion.2
  803.5 2.1 convolution_bitcast_fusion.2
  805.7 2.1 convolution_bitcast_fusion.2
  807.8 1.9 fusion.43
  809.9 20.0 %reduce-scatter.2.cloned.1.call-done = f32[2,8,16,64]{3,2,1,0:T(8,128)} async-done(((f32[2,8,64,64]{3,2,1,0:T(8,128)}), f32[2,8,16,64]{3,2,1,0:T(8,128)}) %reduce-scatter.2.cloned.1.call-update) | async-done | bytes 65552 | tf_op jit(solution)/shard_map/reduce_scatter | solution.py:151
  831.0 8.8 %psum.7 = f32[2,8,64]{2,1,0:T(8,128)S(1)} all-reduce(f32[2,8,64]{2,1,0:T(8,128)S(1)} %bitcast.125), channel_id=1, replica_groups=mesh['grp'=2,'sp'=4,'tp'=4] {'sp'}, use_global_device_ids=true, to_apply=%region_7.8 | all-reduce | flops 1024 | bytes 8192 | tf_op jit(solution)/shard_map/psum | solution.py:156
  (69 shorter events, 29.4 us)
Async XLA Ops:
  7.2 1.0 copy-start
  7.2 794.0 %all-gather.3.cloned.1.call-start = ((), (), s32[]{:S(2)}) async-start(), calls=%async_computation.2 | async-start | bytes 2621440 | tf_op jit(solution)/shard_map/all_gather | solution.py:18
  38.8 1.9 copy-start.4
  691.4 3.4 copy-start.5
  694.9 3.8 copy-start.6
  751.8 0.8 copy-start.2
  752.6 77.3 %reduce-scatter.2.cloned.1.call-start = ((), (), s32[]{:S(2)}) async-start(), calls=%async_computation.1 | async-start | bytes 655360 | tf_op jit(solution)/shard_map/reduce_scatter | solution.py:151
  801.2 6.6 copy-start.3
  801.2 8.5 %copy-start.7 = (bf16[2,512]{1,0:T(2,128)(2,1)S(1)}, bf16[2,512]{1,0:T(2,128)(2,1)}, u32[]{:S(2)}) copy-start(bf16[2,512]{1,0:T(2,128)(2,1)} %param.19) | copy-start | bytes 6148
  807.8 34.4 %copy-start.1 = (bf16[4096,32]{0,1:T(8,128)(2,1)S(1)}, bf16[4096,32]{0,1:T(8,128)(2,1)}, u32[]{:S(2)}) copy-start(bf16[4096,32]{0,1:T(8,128)(2,1)} %param.16) | copy-start | bytes 786436
Sparse Core Ops, SparseCore 0:
  752.8 48.3 all-gather.2
  809.9 19.9 reduce-scatter.1
where the time goes:
time: 851 us; the launch traced here: 849 us
  other arithmetic  647 us (76%)
  matrix products  85.7 us (10%)
  waiting for transfers between devices  68.4 us (8%)
  local copies, waits for them, and re-layouts  24.3 us (3%)
  between operations  14.2 us (2%)
  blocking collectives  8.75 us (1%)
    another operation x1, other arithmetic, block_parts(): solved = jax.scipy.linalg.solve_triangular(lower, right, lower=True)  631 us
    all_gather x1, waiting for transfers between devices, prefix(): gathered = lax.all_gather(part, axis)  48.4 us
    reduce_scatter x1, waiting for transfers between devices, body(): final = lax.psum_scatter(terms, 'sp', scatter_dimension=2, tiled=True)  20 us
    dot_general x8, matrix products, advance(): jnp.einsum('gck,gcw->gkw', carried, fresh, precision=finest)  17.3 us
  transfers between devices with their start and end apart: 2, of which 2 were waited for; matrix products, arithmetic and copies ran while one was open for 0% of the time, Pallas kernels for 0%

commit v1 on v0

v1 whole, which is shorter than its diff:
```python
import functools
import math

import jax
import jax.numpy as jnp
from jax import lax
from jax.experimental import pallas as pl
from jax.experimental.pallas import tpu as pltpu
from jax.sharding import PartitionSpec as P

HEAD = 64
F32 = jnp.float32
BF16 = jnp.bfloat16

finest = lax.Precision.HIGHEST


def mm(left, right):
    return jnp.dot(left, right, preferred_element_type=F32)


def iota(shape, dim):
    return lax.broadcasted_iota(jnp.int32, shape, dim)


def onehot(flag):
    return jnp.where(flag, 1.0, 0.0).astype(BF16)


def lane_masks(pack, width):
    lane_head = iota((1, width), 1) // HEAD
    return [onehot(lane_head == h) for h in range(pack)]


def blockdiag(member, masks):
    return jnp.concatenate([member * mask for mask in masks], axis=0)


def kernel(steps_per_seq, pack, x_ref, wk_ref, wv_ref, wb_ref, wf_ref, speed_ref, extra_ref,
           out_ref, gate_weight, state):
    step = pl.program_id(0)
    rows = x_ref.shape[0]
    columns = wk_ref.shape[1]
    heads = columns // HEAD
    width = pack * HEAD
    quads = columns // width
    chunks = rows // HEAD
    all_heads = wb_ref.shape[1]
    first_head = lax.axis_index("tp") * heads
    masks = lane_masks(pack, width)

    row_c = iota((HEAD, width), 0)
    lane_c = iota((HEAD, width), 1) % HEAD
    below = row_c > lane_c
    diagonal = row_c == lane_c
    apart = row_c ^ lane_c

    @pl.when(step == 0)
    def _():
        source = iota((all_heads, 128), 0)
        lane = iota((all_heads, 128), 1)
        to_beta = onehot((source == first_head + lane) & (lane < heads))
        to_decay = onehot((source == first_head + lane - heads) & (lane >= heads) & (lane < 2 * heads))
        gate_weight[...] = (mm(wb_ref[...], to_beta) + mm(wf_ref[...], to_decay)).astype(BF16)

    @pl.when(lax.rem(step, steps_per_seq) == 0)
    def _():
        eye = jnp.where(diagonal, 1.0, 0.0)
        for quad in range(quads):
            state[quad, :HEAD, :] = jnp.zeros((HEAD, width), F32)
            state[quad, HEAD:, :] = eye

    x = x_ref[...]
    gates = mm(x, gate_weight[...]).astype(BF16)
    key_proj = mm(x, wk_ref[...]).astype(BF16).astype(F32)
    value_proj = mm(x, wv_ref[...]).astype(BF16).astype(F32)

    source = iota((128, columns), 0)
    target = iota((128, columns), 1) // HEAD
    beta_pre = mm(gates, onehot(source == target))
    decay_pre = mm(gates, onehot(source == target + heads))
    source = iota((heads, columns), 0)
    target = iota((heads, columns), 1) // HEAD
    extra = mm(extra_ref[...], onehot(source == target))

    beta = jax.nn.sigmoid(beta_pre)
    softplus = jnp.maximum(decay_pre, 0.0) + jnp.log1p(jnp.exp(-jnp.abs(decay_pre)))
    gamma = speed_ref[...] * softplus + extra
    high = gamma.astype(BF16)
    rest = gamma - high.astype(F32)
    middle = rest.astype(BF16)
    low = (rest - middle.astype(F32)).astype(BF16)
    r_idx = iota((rows, rows), 0)
    c_idx = iota((rows, rows), 1)
    running = onehot((r_idx >= c_idx) & (r_idx // HEAD == c_idx // HEAD))
    cumul = mm(running, high) + mm(running, middle) + mm(running, low)

    key = key_proj * jax.nn.sigmoid(key_proj)
    value = value_proj * jax.nn.sigmoid(value_proj)
    group = onehot(iota((width, width), 0) // HEAD == iota((width, width), 1) // HEAD)
    squares = (key * key).astype(BF16)
    total = jnp.concatenate(
        [mm(squares[:, q * width:(q + 1) * width], group) for q in range(quads)], axis=1)
    key = key * lax.rsqrt(total + 1e-06)

    units = []
    for chunk in range(chunks):
        for quad in range(quads):
            units.append((slice(chunk * HEAD, (chunk + 1) * HEAD), slice(quad * width, (quad + 1) * width)))

    lowers = []
    for rs, cs in units:
        k16 = key[rs, cs].astype(BF16)
        gram = lax.dot_general(k16, blockdiag(k16, masks), (((1,), (1,)), ((), ())),
                               preferred_element_type=F32)
        cum = cumul[rs, cs]
        across = jnp.sum(jnp.where(diagonal, cum, 0.0), axis=0, keepdims=True)
        weights = jnp.exp(jnp.where(below, cum - across, 0.0))
        lowers.append(jnp.where(below, beta[rs, cs] * gram * weights, 0.0))

    inverses = [jnp.where(diagonal, 1.0, jnp.where(apart == 1, -lower, 0.0)) for lower in lowers]
    size = 2
    while size < HEAD:
        inv16 = [inverse.astype(BF16) for inverse in inverses]
        parts = []
        for lower, inverse in zip(lowers, inv16):
            corner = jnp.where((apart >= size) & (apart < 2 * size), lower, 0.0).astype(BF16)
            parts.append(mm(inverse, blockdiag(corner, masks)).astype(BF16))
        inverses = [inverse - mm(part, blockdiag(i16, masks))
                    for inverse, part, i16 in zip(inverses, parts, inv16)]
        size *= 2

    maps = []
    for (rs, cs), inverse in zip(units, inverses):
        i16 = inverse.astype(BF16)
        b, k, cum = beta[rs, cs], key[rs, cs], cumul[rs, cs]
        update = mm(i16, blockdiag((b * value[rs, cs]).astype(BF16), masks))
        mixing = mm(i16, blockdiag((b * jnp.exp(cum) * k).astype(BF16), masks))
        last = cum[HEAD - 1:HEAD, :]
        carried = (k * jnp.exp(last - cum)).astype(BF16)
        contract = (((0,), (0,)), ((), ()))
        offset = lax.dot_general(update.astype(BF16), carried, contract, preferred_element_type=F32)
        erase = lax.dot_general(mixing.astype(BF16), carried, contract, preferred_element_type=F32)
        offset = sum(offset[h * HEAD:(h + 1) * HEAD] * masks[h].astype(F32) for h in range(pack))
        erase = jnp.concatenate(
            [erase[h * HEAD:(h + 1) * HEAD].astype(BF16) * masks[h] for h in range(pack)], axis=0)
        maps.append((jnp.exp(last), erase, offset))

    for quad in range(quads):
        held = state[quad]
        for chunk in range(chunks):
            closing, erase, offset = maps[chunk * quads + quad]
            held = closing * held - mm(held.astype(BF16), erase)
            held = jnp.concatenate([held[:HEAD] + offset, held[HEAD:]], axis=0)
        state[quad] = held

    @pl.when(lax.rem(step, steps_per_seq) == steps_per_seq - 1)
    def _():
        out_ref[0] = state[...]


def device_maps(layer_feed, address_mapping, content_mapping, beta_mapping_matrix,
                forgetting_mapping, logged_fading_speed, extra_forgetting):
    seqs, length, depth = layer_feed.shape
    columns = address_mapping.shape[1]
    heads = columns // HEAD
    pack = math.gcd(heads, 4)
    width = pack * HEAD
    quads = heads // pack
    rows = math.gcd(length, 4 * HEAD)
    per_seq = length // rows
    all_heads = beta_mapping_matrix.shape[1]
    speed = jnp.repeat(-jnp.exp(logged_fading_speed), HEAD)[None, :]
    whole = lambda shape: pl.BlockSpec(shape, lambda i: (0, 0), pipeline_mode=pl.Buffered(1))
    return pl.pallas_call(
        functools.partial(kernel, per_seq, pack),
        grid=(seqs * per_seq,),
        out_shape=jax.ShapeDtypeStruct((seqs, quads, 2 * HEAD, width), F32),
        in_specs=[
            pl.BlockSpec((rows, depth), lambda i: (i, 0)),
            whole((depth, columns)),
            whole((depth, columns)),
            whole((depth, all_heads)),
            whole((depth, all_heads)),
            whole((1, columns)),
            pl.BlockSpec((rows, heads), lambda i: (i, 0)),
        ],
        out_specs=pl.BlockSpec((1, quads, 2 * HEAD, width), lambda i: (i // per_seq, 0, 0, 0)),
        scratch_shapes=[
            pltpu.VMEM((depth, 128), BF16),
            pltpu.VMEM((quads, 2 * HEAD, width), F32),
        ],
        compiler_params=pltpu.CompilerParams(
            dimension_semantics=("arbitrary",), vmem_limit_bytes=56 * 2**20),
    )(layer_feed.reshape(seqs * length, depth), address_mapping, content_mapping,
      beta_mapping_matrix, forgetting_mapping, speed, extra_forgetting.reshape(seqs * length, heads))


def matmul(left, right):
    return jnp.einsum("shij,shjk->shik", left, right, precision=finest)


def suffix_product(part, axis):
    count = lax.axis_size(axis)
    ahead = count - 1 - lax.axis_index(axis)
    gathered = lax.all_gather(part, axis)
    start = jnp.broadcast_to(jnp.eye(HEAD, dtype=F32), part.shape)

    def one(hop, carry):
        return matmul(carry, lax.dynamic_index_in_dim(gathered, count - 1 - hop, 0, False))

    return lax.fori_loop(0, ahead, one, start)


def body(layer_feed, address_mapping, content_mapping, beta_mapping_matrix, forgetting_mapping,
         logged_fading_speed, extra_forgetting, opening_probe):
    seqs = layer_feed.shape[0]
    heads = address_mapping.shape[1] // HEAD
    maps = device_maps(layer_feed, address_mapping, content_mapping, beta_mapping_matrix,
                       forgetting_mapping, logged_fading_speed, extra_forgetting)
    quads, width = maps.shape[1], maps.shape[3]
    maps = maps.reshape(seqs, quads, 2, HEAD, width // HEAD, HEAD)
    maps = maps.transpose(2, 0, 1, 4, 5, 3).reshape(2, seqs, heads, HEAD, HEAD)
    offset, transfer = maps[0], maps[1]
    rows = HEAD // lax.axis_size("sp")
    first_row = lax.axis_index("sp") * rows
    terms = matmul(suffix_product(transfer, "sp"), offset)
    final = lax.psum_scatter(terms, "sp", scatter_dimension=2, tiled=True)
    query = opening_probe.reshape(seqs, heads, HEAD)
    query = lax.dynamic_slice_in_dim(query, first_row, rows, 2).astype(F32)
    read = lax.psum(jnp.einsum("shk,shkv->shv", query, final, precision=finest), "sp")
    read = read * lax.rsqrt(jnp.mean(read * read, axis=-1, keepdims=True) + 1e-06)
    return final.astype(BF16), read.reshape(seqs, heads * HEAD).astype(BF16)


def solution(mesh):
    in_specs = (
        P("grp", "sp", None),
        P(None, "tp"),
        P(None, "tp"),
        P(),
        P(),
        P("tp"),
        P("grp", "sp", "tp"),
        P("grp", "tp"),
    )
    out_specs = (P("grp", "tp", "sp", None), P("grp", "tp"))
    return jax.shard_map(body, mesh=mesh, in_specs=in_specs, out_specs=out_specs, check_vma=False)
```

time: 851 us -> 156 us (0.18)
  other arithmetic: 647 us -> 2.38 us
  matrix products: 85.7 us -> 9.03 us
  Pallas kernels: 0 us -> 41.9 us
  local copies, waits for them, and re-layouts: 24.3 us -> 10.7 us
    another operation x2 -> x0, other arithmetic: 634 us -> none  [the longest x1 631 us: block_parts(): solved = jax.scipy.linalg.solve_triangular(lower, right, lower=True)]
    dot_general x22 -> x1, matrix products: 69.6 us -> 1.09 us  [body(): jnp.einsum('shk,shkv->shv', query, final, precision=finest)]
    pallas_call x0 -> x1, Pallas kernels: none -> 41.9 us  [device_maps(): pl.pallas_call(functools.partial(kernel, per_seq, pack), grid=(seqs * per...]
    mul x4 -> x0, other arithmetic: 10.6 us -> none  [the longest x1 3.84 us: block_parts(): keys * (betas * jnp.exp(cumul))[..., None]]
    squeeze x8 -> x0, local copies, waits for them, and re-layouts: 8.74 us -> none  [run_blocks(): final, _ = lax.scan(advance, start, moved)]
where the time goes in v1:
time: 156 us; the launch traced here: 155 us
  waiting for transfers between devices  68.2 us (44%)
  Pallas kernels  41.9 us (27%)
  between operations  14.1 us (9%)
  local copies, waits for them, and re-layouts  10.7 us (7%)
  matrix products  9.03 us (6%)
  blocking collectives  8.77 us (6%)
  other arithmetic  2.38 us (2%)
    all_gather x1, waiting for transfers between devices, suffix_product(): gathered = lax.all_gather(part, axis)  48.3 us
    pallas_call x1, Pallas kernels, device_maps(): pl.pallas_call(functools.partial(kernel, per_seq, pack), grid=(seqs * per...  41.9 us
    reduce_scatter x1, waiting for transfers between devices, body(): final = lax.psum_scatter(terms, 'sp', scatter_dimension=2, tiled=True)  20 us
    psum x1, blocking collectives, body(): lax.psum(jnp.einsum('shk,shkv->shv', query, final, precision=finest), 'sp')  8.77 us
    dot_general x4, matrix products, matmul(): return jnp.einsum('shij,shjk->shik', left, right, precision=finest)  7.94 us
    unnamed x5, local copies, waits for them, and re-layouts  6.18 us
  transfers between devices with their start and end apart: 2, of which 2 were waited for; matrix products, arithmetic and copies ran while one was open for 0% of the time, Pallas kernels for 0%

profile of v1, /device:TPU:0, one launch (start us, length us, event | category | flops | bytes accessed | tf_op | source)
XLA Modules:
  0.0 155.3 jit_solution(7515677600584201885)
XLA Ops:
  7.2 0.0 all-gather.2.cloned.1.call-start
  7.2 2.3 %copy.19.wb_ref = bf16[4096,32]{1,0:T(8,128)(2,1)} copy(bf16[4096,32]{0,1:T(8,128)(2,1)} %param.13) | data formatting | bytes 524288 | tf_op args[3]
  9.5 2.3 %copy.20.wf_ref = bf16[4096,32]{1,0:T(8,128)(2,1)} copy(bf16[4096,32]{0,1:T(8,128)(2,1)} %param.14) | data formatting | bytes 524288 | tf_op args[4]
  11.8 0.7 exponential_negate_fusion
  12.5 0.1 broadcast_in_dim.8
  12.5 0.7 broadcast_in_dim_reshape.3.speed_ref
  13.2 1.6 %copy.18 = bf16[2,512,8]{2,1,0:T(8,128)(2,1)} copy(bf16[2,512,8]{1,2,0:T(8,128)(2,1)} %param.16) | data formatting | bytes 32768 | tf_op args[6]
  14.8 41.9 %shard_map.95 = f32[2,2,128,256]{3,2,1,0:T(8,128)} custom-call(bf16[1024,4096]{1,0:T(8,128)(2,1)} %bitcast.27, bf16[4096,512]{1,0:T(8,128)(2,1)} %wk_ref.1, bf16[4096,512]{1,0:T(8,128)(2,1)} %wv_ref.1, bf16[4096,32]{1,0:T(8,128)(2,1)} %copy.19.wb_ref, bf16[4096,32]{1,0:T(8,128)(2,1)} %copy.20.wf_ref, f32[1,512]{1,0:T(1,128)} %broadcast_in_dim_reshape.3.speed_ref, ...), custom_call_target="tpu_custom_call" | custom-call | tf_op jit(solution)/shard_map/pallas_call | solution.py:175
  56.7 1.5 reshape.32
  58.1 0.1 fusion.6
  58.2 1.0 copy.21
  59.2 0.0 all-gather.2.cloned.1.call-update
  59.3 0.0 reduce-scatter.2.cloned.1.call-start
  59.3 0.2 copy.23
  59.5 48.3 %all-gather.2.cloned.1.call-done = f32[4,2,8,64,64]{4,3,2,1,0:T(8,128)} async-done(((f32[1,2,8,64,64]{4,3,2,1,0:T(8,128)}), f32[4,2,8,64,64]{4,3,2,1,0:T(8,128)}) %all-gather.2.cloned.1.call-update) | async-done | bytes 1048592 | tf_op jit(solution)/shard_map/all_gather | solution.py:206
  107.8 0.0 copy-start
  107.9 6.4 %while.12 = (s32[]{:T(128)}, f32[2,8,64,64]{2,3,1,0:T(8,128)S(1)}, s32[]{:T(128)}, f32[4,2,8,64,64]{4,3,2,1,0:T(8,128)}, s32[]{:T(128)}, /*index=5*/s32[]{:T(128)}, s32[]{:T(128)}, s32[]{:T(128)}) while((s32[]{:T(128)}, f32[2,8,64,64]{2,3,1,0:T(8,128)S(1)}, s32[]{:T(128)}, f32[4,2,8,64,64]{4,3,2,1,0:T(8,128)}, s32[]{:T(128)}, ...), condition=%wide.region_1.2_spmd, body=%wide.region_0.1_spmd.sunk | while | flops 50331652 | bytes 1573007 | solution.py:212
  107.9 2.0 %convolution_bitcast_fusion.2 = f32[2,8,64,64]{2,3,1,0:T(8,128)S(1)} fusion(f32[2,8,64,64]{2,3,1,0:T(8,128)S(1)} %copy.39, f32[4,2,8,64,64]{4,3,2,1,0:T(8,128)} %get-tuple-element.118, s32[]{:T(128)S(6)} %select_n.12), kind=kOutput, calls=%fused_computation.clone.1 | convolution fusion | flops 50331648 | bytes 1048580 | tf_op jit(solution)/shard_map/while/body/shij,shjk->shik/dot_general | solution.py:200
  110.1 2.1 %convolution_bitcast_fusion.2 = f32[2,8,64,64]{2,3,1,0:T(8,128)S(1)} fusion(f32[2,8,64,64]{2,3,1,0:T(8,128)S(1)} %copy.39, f32[4,2,8,64,64]{4,3,2,1,0:T(8,128)} %get-tuple-element.118, s32[]{:T(128)S(6)} %select_n.12), kind=kOutput, calls=%fused_computation.clone.1 | convolution fusion | flops 50331648 | bytes 1048580 | tf_op jit(solution)/shard_map/while/body/shij,shjk->shik/dot_general | solution.py:200
  112.2 2.0 %convolution_bitcast_fusion.2 = f32[2,8,64,64]{2,3,1,0:T(8,128)S(1)} fusion(f32[2,8,64,64]{2,3,1,0:T(8,128)S(1)} %copy.39, f32[4,2,8,64,64]{4,3,2,1,0:T(8,128)} %get-tuple-element.118, s32[]{:T(128)S(6)} %select_n.12), kind=kOutput, calls=%fused_computation.clone.1 | convolution fusion | flops 50331648 | bytes 1048580 | tf_op jit(solution)/shard_map/while/body/shij,shjk->shik/dot_general | solution.py:200
  114.2 1.8 %fusion.7 = f32[2,8,64,64]{3,2,1,0:T(8,128)} fusion(f32[2,8,64,64]{2,3,1,0:T(8,128)S(1)} %get-tuple-element.58, f32[2,8,64,64]{3,2,1,0:T(8,128)S(1)} %bitcast.29), kind=kOutput, calls=%fused_computation.14 | convolution fusion | flops 50331648 | bytes 786432 | tf_op jit(solution)/shard_map/shij,shjk->shik/dot_general | solution.py:200
  116.0 0.0 reduce-scatter.2.cloned.1.call-update
  116.1 0.0 copy-done
  116.1 0.1 reshape.33
  116.2 0.1 dynamic-slice_bitcast_fusion
  116.2 20.0 %reduce-scatter.2.cloned.1.call-done = f32[2,8,16,64]{3,2,1,0:T(8,128)} async-done(((f32[2,8,64,64]{3,2,1,0:T(8,128)}), f32[2,8,16,64]{3,2,1,0:T(8,128)}) %reduce-scatter.2.cloned.1.call-update) | async-done | bytes 65552 | tf_op jit(solution)/shard_map/reduce_scatter | solution.py:228
  136.2 1.1 fusion.4
  137.3 8.8 %psum.7 = f32[2,8,64]{2,1,0:T(8,128)S(1)} all-reduce(f32[2,8,64]{2,1,0:T(8,128)S(1)} %bitcast.32), channel_id=1, replica_groups=mesh['grp'=2,'sp'=4,'tp'=4] {'sp'}, use_global_device_ids=true, to_apply=%region_3.4 | all-reduce | flops 1024 | bytes 8192 | tf_op jit(solution)/shard_map/psum | solution.py:231
  146.1 0.1 multiply_reduce_fusion
  146.2 0.1 multiply_convert_fusion
  146.2 0.7 convert_element_type.16
  146.9 1.5 convert_element_type.14
  (6 shorter events, 0.2 us)
Async XLA Ops:
  7.2 100.6 %all-gather.2.cloned.1.call-start = ((), (), s32[]{:S(2)}) async-start(), calls=%async_computation.1 | async-start | bytes 2621440 | tf_op jit(solution)/shard_map/all_gather | solution.py:206
  59.3 76.9 %reduce-scatter.2.cloned.1.call-start = ((), (), s32[]{:S(2)}) async-start(), calls=%async_computation.2 | async-start | bytes 655360 | tf_op jit(solution)/shard_map/reduce_scatter | solution.py:228
  107.8 8.2 %copy-start = (bf16[2,512]{1,0:T(2,128)(2,1)S(1)}, bf16[2,512]{1,0:T(2,128)(2,1)}, u32[]{:S(2)}) copy-start(bf16[2,512]{1,0:T(2,128)(2,1)} %param.17) | copy-start | bytes 6148
Sparse Core Ops, SparseCore 0:
  59.4 48.3 all-gather.1
  116.2 19.9 reduce-scatter.1

commit v2 on v1

--- a/solution.py
+++ b/solution.py
@@ -36,16 +36,90 @@
     return jnp.concatenate([member * mask for mask in masks], axis=0)
 
 
-def kernel(steps_per_seq, pack, x_ref, wk_ref, wv_ref, wb_ref, wf_ref, speed_ref, extra_ref,
-           out_ref, gate_weight, state):
-    step = pl.program_id(0)
+def split(member):
+    high = member.astype(BF16)
+    return high, (member - high.astype(F32)).astype(BF16)
+
+
+def finish(masks, pack, sp, units, per, q_ref, ctx_ref, read_ref, maps, arrived, leaving,
+           landed, reads, send_sem, recv_sem, send_out, recv_out):
+    me = lax.axis_index("sp")
+    rows = HEAD // sp
+    width = pack * HEAD
+    lines = width // 128
+    eye = jnp.where(iota((HEAD, width), 0) == iota((HEAD, width), 1) % HEAD, 1.0, 0.0)
+    head_row = iota((8, width), 0)
+    head_lane = iota((8, width), 1) // HEAD
+    for i in range(per):
+        for d in range(1, sp):
+            peer_copy(maps.at[0], arrived.at[lax.rem(me + sp - d, sp), i], send_sem.at[0],
+                      recv_sem.at[i, d], me).wait_recv()
+        final = arrived[0, i, :HEAD, :]
+        for j in range(1, sp):
+            high, low = split(final)
+            t_high, t_low = split(arrived[j, i, HEAD:, :])
+            t_high = blockdiag(t_high, masks)
+            final = (mm(high, t_high) + mm(low, t_high) + mm(high, blockdiag(t_low, masks))
+                     + arrived[j, i, :HEAD, :])
+        query = jnp.where(head_row == head_lane, q_ref[me * per + i], 0.0)
+        read = lax.dot_general(query, final, (((1,), (1,)), ((), ())), precision=finest,
+                               preferred_element_type=F32)
+        read = read * lax.rsqrt(jnp.mean(read * read, axis=1, keepdims=True) + 1e-06)
+        read = jnp.dot(read, eye, precision=finest, preferred_element_type=F32)
+        read = jnp.sum(jnp.where(head_row == head_lane, read, 0.0), axis=0, keepdims=True)
+        turned = final.T
+        for j in range(sp):
+            for h in range(pack):
+                leaving[i, j, h * rows:(h + 1) * rows, :HEAD] = (
+                    turned[h * HEAD + j * rows:h * HEAD + (j + 1) * rows, :])
+            for line in range(lines):
+                leaving[i, j, pack * rows + line:pack * rows + line + 1, :] = (
+                    read[:, line * 128:(line + 1) * 128])
+        for d in range(1, sp):
+            peer = lax.rem(me + d, sp)
+            peer_copy(leaving.at[i, peer], landed.at[me * per + i], send_out.at[i, d],
+                      recv_out.at[i, d], peer).start()
+        landed[me * per + i] = leaving[i, me]
+    for i in range(per):
+        for d in range(1, sp):
+            peer = lax.rem(me + sp - d, sp)
+            peer_copy(leaving.at[i, 0], landed.at[peer * per + i], send_out.at[i, d],
+                      recv_out.at[i, d], peer).wait_recv()
+    quads = reads.shape[1] // width
+    for u in range(units):
+        ctx_ref[u] = landed[u, :pack * rows, :HEAD].astype(BF16)
+        for line in range(lines):
+            at = (u % quads) * width + line * 128
+            reads[u // quads:u // quads + 1, at:at + 128] = (
+                landed[u, pack * rows + line:pack * rows + line + 1, :])
+    read_ref[...] = reads[...].astype(BF16)
+    for i in range(per):
+        for d in range(1, sp):
+            peer = lax.rem(me + d, sp)
+            peer_copy(leaving.at[i, peer], landed.at[me * per + i], send_out.at[i, d],
+                      recv_out.at[i, d], peer).wait_send()
+    for u in range(units):
+        @pl.when(u // per != me)
+        def _():
+            peer_copy(maps.at[u], arrived.at[me, u % per], send_sem.at[u],
+                      recv_sem.at[u % per, 0], u // per).wait_send()
+
+
+def peer_copy(source, target, send_sem, recv_sem, peer):
+    return pltpu.make_async_remote_copy(
+        src_ref=source, dst_ref=target, send_sem=send_sem, recv_sem=recv_sem,
+        device_id={"sp": peer}, device_id_type=pl.DeviceIdType.MESH)
+
+
+def local_stage(step, steps_per_seq, pack, x_ref, wk_ref, wv_ref, wb_ref, wf_ref, speed_ref,
+                extra_ref, gate_weight, state):
     rows = x_ref.shape[0]
     columns = wk_ref.shape[1]
     heads = columns // HEAD
     width = pack * HEAD
     quads = columns // width
     chunks = rows // HEAD
-    all_heads = wb_ref.shape[1]
+    all_heads = wb_ref.shape[0]
     first_head = lax.axis_index("tp") * heads
     masks = lane_masks(pack, width)
 
@@ -57,11 +131,11 @@
 
     @pl.when(step == 0)
     def _():
-        source = iota((all_heads, 128), 0)
-        lane = iota((all_heads, 128), 1)
+        source = iota((128, all_heads), 1)
+        lane = iota((128, all_heads), 0)
         to_beta = onehot((source == first_head + lane) & (lane < heads))
         to_decay = onehot((source == first_head + lane - heads) & (lane >= heads) & (lane < 2 * heads))
-        gate_weight[...] = (mm(wb_ref[...], to_beta) + mm(wf_ref[...], to_decay)).astype(BF16)
+        gate_weight[...] = (mm(to_beta, wb_ref[...]) + mm(to_decay, wf_ref[...])).astype(BF16)
 
     @pl.when(lax.rem(step, steps_per_seq) == 0)
     def _():
@@ -71,7 +145,8 @@
             state[quad, HEAD:, :] = eye
 
     x = x_ref[...]
-    gates = mm(x, gate_weight[...]).astype(BF16)
+    gates = lax.dot_general(x, gate_weight[...], (((1,), (1,)), ((), ())),
+                            preferred_element_type=F32).astype(BF16)
     key_proj = mm(x, wk_ref[...]).astype(BF16).astype(F32)
     value_proj = mm(x, wv_ref[...]).astype(BF16).astype(F32)
 
@@ -85,7 +160,9 @@
 
     beta = jax.nn.sigmoid(beta_pre)
     softplus = jnp.maximum(decay_pre, 0.0) + jnp.log1p(jnp.exp(-jnp.abs(decay_pre)))
-    gamma = speed_ref[...] * softplus + extra
+    speed = jnp.dot(-jnp.exp(speed_ref[...]), jnp.where(source == target, 1.0, 0.0),
+                    precision=finest, preferred_element_type=F32)
+    gamma = speed * softplus + extra
     high = gamma.astype(BF16)
     rest = gamma - high.astype(F32)
     middle = rest.astype(BF16)
@@ -154,9 +231,130 @@
             held = jnp.concatenate([held[:HEAD] + offset, held[HEAD:]], axis=0)
         state[quad] = held
 
+def local_kernel(steps_per_seq, pack, x_ref, wk_ref, wv_ref, wb_ref, wf_ref, speed_ref, extra_ref,
+                 out_ref, gate_weight, state):
+    step = pl.program_id(0)
+    local_stage(step, steps_per_seq, pack, x_ref, wk_ref, wv_ref, wb_ref, wf_ref, speed_ref, extra_ref,
+                gate_weight, state)
+
     @pl.when(lax.rem(step, steps_per_seq) == steps_per_seq - 1)
     def _():
         out_ref[0] = state[...]
+
+
+def kernel(steps_per_seq, pack, sp, x_ref, wk_ref, wv_ref, wb_ref, wf_ref, speed_ref, extra_ref,
+           q_ref, ctx_ref, read_ref, gate_weight, state, maps, arrived, leaving, landed, reads,
+           send_sem, recv_sem, send_out, recv_out):
+    step = pl.program_id(0)
+    steps = pl.num_programs(0)
+    me = lax.axis_index("sp")
+    width = pack * HEAD
+    quads = state.shape[0]
+    masks = lane_masks(pack, width)
+
+    @pl.when(step == 0)
+    def _():
+        barrier = pltpu.get_barrier_semaphore()
+        for d in range(1, sp):
+            pl.semaphore_signal(barrier, inc=1, device_id={"sp": lax.rem(me + d, sp)},
+                                device_id_type=pl.DeviceIdType.MESH)
+
+    local_stage(step, steps_per_seq, pack, x_ref, wk_ref, wv_ref, wb_ref, wf_ref, speed_ref, extra_ref,
+                gate_weight, state)
+    units_all = maps.shape[0]
+    per = units_all // sp
+
+    @pl.when(step == steps_per_seq - 1)
+    def _():
+        pl.semaphore_wait(pltpu.get_barrier_semaphore(), sp - 1)
+
+    @pl.when(lax.rem(step, steps_per_seq) == steps_per_seq - 1)
+    def _():
+        seqs = units_all // quads
+        seq = lax.rem(step // steps_per_seq + me * per // quads + 1, seqs)
+        for quad in range(quads):
+            unit = seq * quads + quad
+            owner = unit // per
+            slot = lax.rem(unit, per)
+
+            @pl.when(owner != me)
+            def _():
+                maps[unit] = state[quad]
+                away = lax.rem(owner - me + sp, sp)
+                peer_copy(maps.at[unit], arrived.at[me, slot], send_sem.at[unit],
+                          recv_sem.at[slot, away], owner).start()
+
+            @pl.when(owner == me)
+            def _():
+                arrived[me, slot] = state[quad]
+
+    @pl.when(step == steps - 1)
+    def _():
+        finish(masks, pack, sp, units_all, per, q_ref, ctx_ref, read_ref, maps, arrived,
+               leaving, landed, reads, send_sem, recv_sem, send_out, recv_out)
+
+
+def fused(layer_feed, address_mapping, content_mapping, beta_mapping_matrix, forgetting_mapping,
+          logged_fading_speed, extra_forgetting, opening_probe):
+    seqs, length, depth = layer_feed.shape
+    columns = address_mapping.shape[1]
+    heads = columns // HEAD
+    pack = math.gcd(heads, 4)
+    width = pack * HEAD
+    quads = heads // pack
+    units = seqs * quads
+    sp = lax.axis_size("sp")
+    per = units // sp
+    rows = math.gcd(length, 4 * HEAD)
+    per_seq = length // rows
+    steps = seqs * per_seq
+    all_heads = beta_mapping_matrix.shape[1]
+    own_rows = HEAD // sp
+    tall = -(-(pack * own_rows + width // 128) // 8) * 8
+    whole = lambda shape: pl.BlockSpec(shape, lambda i: (0,) * len(shape), pipeline_mode=pl.Buffered(1))
+
+    def turn(i):
+        own = lax.axis_index("sp") * per // quads
+        return (lax.rem(i + (own + 1) * per_seq, steps), 0)
+
+    context, read = pl.pallas_call(
+        functools.partial(kernel, per_seq, pack, sp),
+        grid=(steps,),
+        out_shape=(jax.ShapeDtypeStruct((units, pack * own_rows, HEAD), BF16),
+                   jax.ShapeDtypeStruct((seqs, columns), BF16)),
+        in_specs=[
+            pl.BlockSpec((rows, depth), turn),
+            whole((depth, columns)),
+            whole((depth, columns)),
+            whole((all_heads, depth)),
+            whole((all_heads, depth)),
+            whole((1, heads)),
+            pl.BlockSpec((rows, heads), turn),
+            whole((units, 1, width)),
+        ],
+        out_specs=(pl.BlockSpec((units, pack * own_rows, HEAD), lambda i: (0, 0, 0)),
+                   pl.BlockSpec((seqs, columns), lambda i: (0, 0))),
+        scratch_shapes=[
+            pltpu.VMEM((128, depth), BF16),
+            pltpu.VMEM((quads, 2 * HEAD, width), F32),
+            pltpu.VMEM((units, 2 * HEAD, width), F32),
+            pltpu.VMEM((sp, per, 2 * HEAD, width), F32),
+            pltpu.VMEM((per, sp, tall, 128), F32),
+            pltpu.VMEM((units, tall, 128), F32),
+            pltpu.VMEM((seqs, columns), F32),
+            pltpu.SemaphoreType.DMA((units,)),
+            pltpu.SemaphoreType.DMA((per, sp)),
+            pltpu.SemaphoreType.DMA((per, sp)),
+            pltpu.SemaphoreType.DMA((per, sp)),
+        ],
+        compiler_params=pltpu.CompilerParams(
+            dimension_semantics=("arbitrary",), vmem_limit_bytes=56 * 2**20,
+            collective_id=0, has_side_effects=True),
+    )(layer_feed.reshape(seqs * length, depth), address_mapping, content_mapping,
+      beta_mapping_matrix.T, forgetting_mapping.T, logged_fading_speed[None, :],
+      extra_forgetting.reshape(seqs * length, heads),
+      opening_probe.reshape(units, 1, width).astype(F32))
+    return context.reshape(seqs, heads, own_rows, HEAD), read
 
 
 def device_maps(layer_feed, address_mapping, content_mapping, beta_mapping_matrix,
@@ -170,30 +368,29 @@
     rows = math.gcd(length, 4 * HEAD)
     per_seq = length // rows
     all_heads = beta_mapping_matrix.shape[1]
-    speed = jnp.repeat(-jnp.exp(logged_fading_speed), HEAD)[None, :]
     whole = lambda shape: pl.BlockSpec(shape, lambda i: (0, 0), pipeline_mode=pl.Buffered(1))
     return pl.pallas_call(
-        functools.partial(kernel, per_seq, pack),
+        functools.partial(local_kernel, per_seq, pack),
         grid=(seqs * per_seq,),
         out_shape=jax.ShapeDtypeStruct((seqs, quads, 2 * HEAD, width), F32),
         in_specs=[
             pl.BlockSpec((rows, depth), lambda i: (i, 0)),
             whole((depth, columns)),
             whole((depth, columns)),
-            whole((depth, all_heads)),
-            whole((depth, all_heads)),
-            whole((1, columns)),
+            whole((all_heads, depth)),
+            whole((all_heads, depth)),
+            whole((1, heads)),
             pl.BlockSpec((rows, heads), lambda i: (i, 0)),
         ],
         out_specs=pl.BlockSpec((1, quads, 2 * HEAD, width), lambda i: (i // per_seq, 0, 0, 0)),
         scratch_shapes=[
-            pltpu.VMEM((depth, 128), BF16),
+            pltpu.VMEM((128, depth), BF16),
             pltpu.VMEM((quads, 2 * HEAD, width), F32),
         ],
         compiler_params=pltpu.CompilerParams(
             dimension_semantics=("arbitrary",), vmem_limit_bytes=56 * 2**20),
     )(layer_feed.reshape(seqs * length, depth), address_mapping, content_mapping,
-      beta_mapping_matrix, forgetting_mapping, speed, extra_forgetting.reshape(seqs * length, heads))
+      beta_mapping_matrix.T, forgetting_mapping.T, logged_fading_speed[None, :], extra_forgetting.reshape(seqs * length, heads))
 
 
 def matmul(left, right):
@@ -216,6 +413,11 @@
          logged_fading_speed, extra_forgetting, opening_probe):
     seqs = layer_feed.shape[0]
     heads = address_mapping.shape[1] // HEAD
+    sp = lax.axis_size("sp")
+    pack = math.gcd(heads, 4)
+    if pack > 1 and (seqs * heads // pack) % sp == 0 and HEAD % (8 * sp) == 0:
+        return fused(layer_feed, address_mapping, content_mapping, beta_mapping_matrix,
+                     forgetting_mapping, logged_fading_speed, extra_forgetting, opening_probe)
     maps = device_maps(layer_feed, address_mapping, content_mapping, beta_mapping_matrix,
                        forgetting_mapping, logged_fading_speed, extra_forgetting)
     quads, width = maps.shape[1], maps.shape[3]

time: 156 us -> 58.9 us (0.38)
  waiting for transfers between devices: 68.2 us -> 0 us
  between operations: 14.1 us -> 0.64 us
  Pallas kernels: 41.9 us -> 52.4 us
  matrix products: 9.03 us -> 0 us
  blocking collectives: 8.77 us -> 0 us
  local copies, waits for them, and re-layouts: 10.7 us -> 5.56 us
  other arithmetic: 2.38 us -> 0 us
    all_gather x1 -> x0, waiting for transfers between devices: 48.3 us -> none  [suffix_product(): gathered = lax.all_gather(part, axis)]
    reduce_scatter x1 -> x0, waiting for transfers between devices: 20 us -> none  [body(): final = lax.psum_scatter(terms, 'sp', scatter_dimension=2, tiled=True)]
    pallas_call x1, Pallas kernels: 41.9 us -> 52.4 us  [fused(): pl.pallas_call(functools.partial(kernel, per_seq, pack, sp), grid=(steps,...]
    dot_general x5 -> x0, matrix products: 9.03 us -> none  [the longest x4 7.94 us: matmul(): return jnp.einsum('shij,shjk->shik', left, right, precision=finest)]
    psum x1 -> x0, blocking collectives: 8.77 us -> none  [body(): lax.psum(jnp.einsum('shk,shkv->shv', query, final, precision=finest), 'sp')]
    unnamed x5 -> x3, local copies, waits for them, and re-layouts: 6.18 us -> 4.28 us
    convert_element_type x3 -> x0, other arithmetic: 1.62 us -> none  [the longest x2 1.62 us: body(): return (final.astype(BF16), read.reshape(seqs, heads * HEAD).astype(BF16))]
    reshape x2 -> x0, local copies, waits for them, and re-layouts: 1.56 us -> none  [the longest x1 1.48 us: body(): maps = maps.reshape(seqs, quads, 2, HEAD, width // HEAD, HEAD)]
  transfers between devices with their start and end apart: 2 -> 0, of which waited for: 2 -> 0; matrix products, arithmetic and copies ran while one was open for 0% -> 0% of each run, Pallas kernels for 0% -> 0%
where the time goes in v2:
time: 58.9 us; the launch traced here: 58.6 us
  Pallas kernels  52.4 us (89%)
  local copies, waits for them, and re-layouts  5.56 us (9%)
  between operations  0.64 us (1%)
    pallas_call x1, Pallas kernels, fused(): pl.pallas_call(functools.partial(kernel, per_seq, pack, sp), grid=(steps,...  52.4 us
    unnamed x3, local copies, waits for them, and re-layouts  4.28 us
    convert_element_type x1, local copies, waits for them, and re-layouts, fused(): opening_probe.reshape(units, 1, width).astype(F32)  1.28 us

profile of v2, /device:TPU:0, one launch (start us, length us, event | category | flops | bytes accessed | tf_op | source)
XLA Modules:
  0.0 58.6 jit_solution(4509744276814787556)
XLA Ops:
  0.6 1.3 %reshape.31.q_ref = f32[4,1,256]{2,1,0:T(1,128)} reshape(bf16[2,512]{1,0:T(2,128)(2,1)} %param.15) | data formatting | bytes 6144 | tf_op jit(solution)/shard_map/convert_element_type | solution.py:356
  1.9 1.5 %copy.10 = bf16[2,512,8]{2,1,0:T(8,128)(2,1)} copy(bf16[2,512,8]{1,2,0:T(8,128)(2,1)} %param.14) | data formatting | bytes 32768 | tf_op args[6]
  3.5 52.4 %shard_map.95 = (bf16[4,64,64]{2,1,0:T(8,128)(2,1)}, bf16[2,512]{1,0:T(2,128)(2,1)}) custom-call(bf16[1024,4096]{1,0:T(8,128)(2,1)} %bitcast.6, bf16[4096,512]{1,0:T(8,128)(2,1)} %wk_ref.1, bf16[4096,512]{1,0:T(8,128)(2,1)} %wv_ref.1, bf16[32,4096]{1,0:T(8,128)(2,1)} %bitcast.8, bf16[32,4096]{1,0:T(8,128)(2,1)} %bitcast.9, f32[1,8]{1,0:T(1,128)} %bitcast.11, ...), custom_call_target="tpu_custom_call" | custom-call | tf_op jit(solution)/shard_map/pallas_call | solution.py:320
  55.9 1.5 %copy.13 = bf16[2,8,16,64]{3,2,1,0:T(8,128)(2,1)} copy(bf16[2,8,16,64]{3,2,1,0:T(8,128)(2,1)} %bitcast.10) | data formatting | bytes 65536
  57.4 1.3 %copy.14 = bf16[2,512]{1,0:T(2,128)(2,1)} copy(bf16[2,512]{1,0:T(2,128)(2,1)} %get-tuple-element.9) | data formatting | bytes 4096

commit v3 on v2

--- a/solution.py
+++ b/solution.py
@@ -28,12 +28,22 @@
 
 
 def lane_masks(pack, width):
-    lane_head = iota((1, width), 1) // HEAD
-    return [onehot(lane_head == h) for h in range(pack)]
+    tile = min(128, width)
+    lane_head = iota((1, tile), 1) // HEAD
+    return [onehot(lane_head == h) for h in range(tile // HEAD)]
 
 
 def blockdiag(member, masks):
-    return jnp.concatenate([member * mask for mask in masks], axis=0)
+    width = member.shape[1]
+    tile = masks[0].shape[1]
+    zeros = jnp.zeros((member.shape[0], tile), member.dtype)
+    lines = []
+    for head in range(width // HEAD):
+        place = head * HEAD // tile
+        pieces = [zeros] * (width // tile)
+        pieces[place] = member[:, place * tile:(place + 1) * tile] * masks[head % len(masks)]
+        lines.append(jnp.concatenate(pieces, axis=1))
+    return jnp.concatenate(lines, axis=0)
 
 
 def split(member):
@@ -48,6 +58,8 @@
     width = pack * HEAD
     lines = width // 128
     eye = jnp.where(iota((HEAD, width), 0) == iota((HEAD, width), 1) % HEAD, 1.0, 0.0)
+    quads = reads.shape[1] // width
+    probe = q_ref[...].astype(F32)
     head_row = iota((8, width), 0)
     head_lane = iota((8, width), 1) // HEAD
     for i in range(per):
@@ -61,7 +73,12 @@
             t_high = blockdiag(t_high, masks)
             final = (mm(high, t_high) + mm(low, t_high) + mm(high, blockdiag(t_low, masks))
                      + arrived[j, i, :HEAD, :])
-        query = jnp.where(head_row == head_lane, q_ref[me * per + i], 0.0)
+        query = jnp.zeros((1, width), F32)
+        for u in range(i, units, per):
+            mine = jnp.where(u == me * per + i, 1.0, 0.0)
+            at = (u % quads) * width
+            query = query + mine * probe[u // quads:u // quads + 1, at:at + width]
+        query = jnp.where(head_row == head_lane, query, 0.0)
         read = lax.dot_general(query, final, (((1,), (1,)), ((), ())), precision=finest,
                                preferred_element_type=F32)
         read = read * lax.rsqrt(jnp.mean(read * read, axis=1, keepdims=True) + 1e-06)
@@ -85,7 +102,6 @@
             peer = lax.rem(me + sp - d, sp)
             peer_copy(leaving.at[i, 0], landed.at[peer * per + i], send_out.at[i, d],
                       recv_out.at[i, d], peer).wait_recv()
-    quads = reads.shape[1] // width
     for u in range(units):
         ctx_ref[u] = landed[u, :pack * rows, :HEAD].astype(BF16)
         for line in range(lines):
@@ -156,7 +172,8 @@
     decay_pre = mm(gates, onehot(source == target + heads))
     source = iota((heads, columns), 0)
     target = iota((heads, columns), 1) // HEAD
-    extra = mm(extra_ref[...], onehot(source == target))
+    extra = lax.dot_general(extra_ref[0], onehot(source == target), (((0,), (0,)), ((), ())),
+                            preferred_element_type=F32)
 
     beta = jax.nn.sigmoid(beta_pre)
     softplus = jnp.maximum(decay_pre, 0.0) + jnp.log1p(jnp.exp(-jnp.abs(decay_pre)))
@@ -185,51 +202,72 @@
         for quad in range(quads):
             units.append((slice(chunk * HEAD, (chunk + 1) * HEAD), slice(quad * width, (quad + 1) * width)))
 
+    grown = jnp.exp(cumul)
+    key16 = key.astype(BF16)
+    weighted_key = (beta * grown * key).astype(BF16)
+    weighted_value = (beta * value).astype(BF16)
+    tile = masks[0].shape[1]
+    eye16 = onehot(diagonal)
+    levels = [onehot((apart >= 1 << p) & (apart < 2 << p)) for p in range(HEAD.bit_length() - 1)]
+    contract = (((0,), (0,)), ((), ()))
+
+    grams = []
+    for rs, cs in units:
+        grams.append(lax.dot_general(key16[rs, cs], blockdiag(key16[rs, cs], masks),
+                                     (((1,), (1,)), ((), ())), preferred_element_type=F32))
     lowers = []
-    for rs, cs in units:
-        k16 = key[rs, cs].astype(BF16)
-        gram = lax.dot_general(k16, blockdiag(k16, masks), (((1,), (1,)), ((), ())),
-                               preferred_element_type=F32)
+    for (rs, cs), gram in zip(units, grams):
         cum = cumul[rs, cs]
         across = jnp.sum(jnp.where(diagonal, cum, 0.0), axis=0, keepdims=True)
-        weights = jnp.exp(jnp.where(below, cum - across, 0.0))
-        lowers.append(jnp.where(below, beta[rs, cs] * gram * weights, 0.0))
-
-    inverses = [jnp.where(diagonal, 1.0, jnp.where(apart == 1, -lower, 0.0)) for lower in lowers]
-    size = 2
-    while size < HEAD:
-        inv16 = [inverse.astype(BF16) for inverse in inverses]
-        parts = []
-        for lower, inverse in zip(lowers, inv16):
-            corner = jnp.where((apart >= size) & (apart < 2 * size), lower, 0.0).astype(BF16)
-            parts.append(mm(inverse, blockdiag(corner, masks)).astype(BF16))
-        inverses = [inverse - mm(part, blockdiag(i16, masks))
-                    for inverse, part, i16 in zip(inverses, parts, inv16)]
-        size *= 2
-
-    maps = []
-    for (rs, cs), inverse in zip(units, inverses):
-        i16 = inverse.astype(BF16)
-        b, k, cum = beta[rs, cs], key[rs, cs], cumul[rs, cs]
-        update = mm(i16, blockdiag((b * value[rs, cs]).astype(BF16), masks))
-        mixing = mm(i16, blockdiag((b * jnp.exp(cum) * k).astype(BF16), masks))
-        last = cum[HEAD - 1:HEAD, :]
-        carried = (k * jnp.exp(last - cum)).astype(BF16)
-        contract = (((0,), (0,)), ((), ()))
-        offset = lax.dot_general(update.astype(BF16), carried, contract, preferred_element_type=F32)
-        erase = lax.dot_general(mixing.astype(BF16), carried, contract, preferred_element_type=F32)
-        offset = sum(offset[h * HEAD:(h + 1) * HEAD] * masks[h].astype(F32) for h in range(pack))
-        erase = jnp.concatenate(
-            [erase[h * HEAD:(h + 1) * HEAD].astype(BF16) * masks[h] for h in range(pack)], axis=0)
-        maps.append((jnp.exp(last), erase, offset))
-
+        weights = jnp.exp(jnp.where(below, cum - across, -1e30))
+        lowers.append((beta[rs, cs] * gram * weights).astype(BF16))
+
+    inverses = [eye16 - lower * levels[0] for lower in lowers]
+    for level in levels[1:]:
+        parts = [mm(inverse, blockdiag(lower * level, masks)).astype(BF16)
+                 for lower, inverse in zip(lowers, inverses)]
+        inverses = [inverse - mm(part, blockdiag(inverse, masks)).astype(BF16)
+                    for inverse, part in zip(inverses, parts)]
+
+    updates = [mm(inverse, blockdiag(weighted_value[rs, cs], masks)).astype(BF16)
+               for (rs, cs), inverse in zip(units, inverses)]
+    mixings = [mm(inverse, blockdiag(weighted_key[rs, cs], masks)).astype(BF16)
+               for (rs, cs), inverse in zip(units, inverses)]
+    closings, erases, offsets = [], [], []
+    upper_lanes = iota((HEAD, tile), 1) >= HEAD
+    for (rs, cs), update, mixing in zip(units, updates, mixings):
+        last = cumul[rs, cs][HEAD - 1:HEAD, :]
+        carried = (key[rs, cs] * jnp.exp(last - cumul[rs, cs])).astype(BF16)
+        closings.append(jnp.exp(last))
+        offset_tiles, erase_lines = [], []
+        zeros = jnp.zeros((tile, tile), BF16)
+        for place in range(width // tile):
+            ts = slice(place * tile, (place + 1) * tile)
+            offset = lax.dot_general(update[:, ts], carried[:, ts], contract, preferred_element_type=F32)
+            erase = lax.dot_general(mixing[:, ts], carried[:, ts], contract, preferred_element_type=F32)
+            if tile > HEAD:
+                offset = jnp.where(upper_lanes, offset[HEAD:], offset[:HEAD])
+            offset_tiles.append(offset)
+            erase = erase.astype(BF16)
+            erase = jnp.concatenate(
+                [erase[h * HEAD:(h + 1) * HEAD] * masks[h] for h in range(tile // HEAD)], axis=0)
+            line = [zeros] * (width // tile)
+            line[place] = erase
+            erase_lines.append(jnp.concatenate(line, axis=1))
+        offsets.append(jnp.concatenate(offset_tiles, axis=1))
+        erases.append(jnp.concatenate(erase_lines, axis=0))
+
+    held = [(state[quad, :HEAD, :], state[quad, HEAD:, :]) for quad in range(quads)]
+    for chunk in range(chunks):
+        for quad in range(quads):
+            u = chunk * quads + quad
+            above, under = held[quad]
+            erased = mm(jnp.concatenate([above, under], axis=0).astype(BF16), erases[u])
+            held[quad] = (closings[u] * above - erased[:HEAD] + offsets[u],
+                          closings[u] * under - erased[HEAD:])
     for quad in range(quads):
-        held = state[quad]
-        for chunk in range(chunks):
-            closing, erase, offset = maps[chunk * quads + quad]
-            held = closing * held - mm(held.astype(BF16), erase)
-            held = jnp.concatenate([held[:HEAD] + offset, held[HEAD:]], axis=0)
-        state[quad] = held
+        state[quad, :HEAD, :], state[quad, HEAD:, :] = held[quad]
+
 
 def local_kernel(steps_per_seq, pack, x_ref, wk_ref, wv_ref, wb_ref, wf_ref, speed_ref, extra_ref,
                  out_ref, gate_weight, state):
@@ -317,6 +355,10 @@
         own = lax.axis_index("sp") * per // quads
         return (lax.rem(i + (own + 1) * per_seq, steps), 0)
 
+    def turn_extra(i):
+        block = turn(i)[0]
+        return (block // per_seq, 0, lax.rem(block, per_seq))
+
     context, read = pl.pallas_call(
         functools.partial(kernel, per_seq, pack, sp),
         grid=(steps,),
@@ -329,8 +371,8 @@
             whole((all_heads, depth)),
             whole((all_heads, depth)),
             whole((1, heads)),
-            pl.BlockSpec((rows, heads), turn),
-            whole((units, 1, width)),
+            pl.BlockSpec((1, heads, rows), turn_extra),
+            whole((seqs, columns)),
         ],
         out_specs=(pl.BlockSpec((units, pack * own_rows, HEAD), lambda i: (0, 0, 0)),
                    pl.BlockSpec((seqs, columns), lambda i: (0, 0))),
@@ -352,8 +394,8 @@
             collective_id=0, has_side_effects=True),
     )(layer_feed.reshape(seqs * length, depth), address_mapping, content_mapping,
       beta_mapping_matrix.T, forgetting_mapping.T, logged_fading_speed[None, :],
-      extra_forgetting.reshape(seqs * length, heads),
-      opening_probe.reshape(units, 1, width).astype(F32))
+      extra_forgetting.transpose(0, 2, 1),
+      opening_probe)
     return context.reshape(seqs, heads, own_rows, HEAD), read
 
 
@@ -380,7 +422,7 @@
             whole((all_heads, depth)),
             whole((all_heads, depth)),
             whole((1, heads)),
-            pl.BlockSpec((rows, heads), lambda i: (i, 0)),
+            pl.BlockSpec((1, heads, rows), lambda i: (i // per_seq, 0, i % per_seq)),
         ],
         out_specs=pl.BlockSpec((1, quads, 2 * HEAD, width), lambda i: (i // per_seq, 0, 0, 0)),
         scratch_shapes=[
@@ -390,7 +432,7 @@
         compiler_params=pltpu.CompilerParams(
             dimension_semantics=("arbitrary",), vmem_limit_bytes=56 * 2**20),
     )(layer_feed.reshape(seqs * length, depth), address_mapping, content_mapping,
-      beta_mapping_matrix.T, forgetting_mapping.T, logged_fading_speed[None, :], extra_forgetting.reshape(seqs * length, heads))
+      beta_mapping_matrix.T, forgetting_mapping.T, logged_fading_speed[None, :], extra_forgetting.transpose(0, 2, 1))
 
 
 def matmul(left, right):

time: 58.9 us -> 48.9 us (0.83)
  Pallas kernels: 52.4 us -> 45.4 us
  local copies, waits for them, and re-layouts: 5.56 us -> 2.72 us
    pallas_call x1, Pallas kernels: 52.4 us -> 45.4 us  [fused(): pl.pallas_call(functools.partial(kernel, per_seq, pack, sp), grid=(steps,...]
    unnamed x3 -> x2, local copies, waits for them, and re-layouts: 4.28 us -> 2.72 us
    convert_element_type x1 -> x0, local copies, waits for them, and re-layouts: 1.28 us -> none  [fused(): opening_probe.reshape(units, 1, width).astype(F32)]
where the time goes in v3:
time: 48.9 us; the launch traced here: 48.7 us
  Pallas kernels  45.4 us (93%)
  local copies, waits for them, and re-layouts  2.72 us (6%)
  between operations  0.64 us (1%)
    pallas_call x1, Pallas kernels, fused(): pl.pallas_call(functools.partial(kernel, per_seq, pack, sp), grid=(steps,...  45.4 us
    unnamed x2, local copies, waits for them, and re-layouts  2.72 us

profile of v3, /device:TPU:0, one launch (start us, length us, event | category | flops | bytes accessed | tf_op | source)
XLA Modules:
  0.0 48.7 jit_solution(12180819741562223565)
XLA Ops:
  0.6 45.4 %shard_map.95 = (bf16[4,64,64]{2,1,0:T(8,128)(2,1)}, bf16[2,512]{1,0:T(2,128)(2,1)}) custom-call(bf16[1024,4096]{1,0:T(8,128)(2,1)} %bitcast.6, bf16[4096,512]{1,0:T(8,128)(2,1)} %wk_ref.1, bf16[4096,512]{1,0:T(8,128)(2,1)} %wv_ref.1, bf16[32,4096]{1,0:T(8,128)(2,1)} %bitcast.7, bf16[32,4096]{1,0:T(8,128)(2,1)} %bitcast.8, f32[1,8]{1,0:T(1,128)} %bitcast.11, ...), custom_call_target="tpu_custom_call" | custom-call | tf_op jit(solution)/shard_map/pallas_call | solution.py:362
  46.0 1.5 %copy.12 = bf16[2,8,16,64]{3,2,1,0:T(8,128)(2,1)} copy(bf16[2,8,16,64]{3,2,1,0:T(8,128)(2,1)} %bitcast.9) | data formatting | bytes 65536
  47.5 1.2 %copy.13 = bf16[2,512]{1,0:T(2,128)(2,1)} copy(bf16[2,512]{1,0:T(2,128)(2,1)} %get-tuple-element.9) | data formatting | bytes 4096

commit v4 on v3

--- a/solution.py
+++ b/solution.py
@@ -49,6 +49,11 @@
 def split(member):
     high = member.astype(BF16)
     return high, (member - high.astype(F32)).astype(BF16)
+
+
+def thirds(member):
+    high = member.astype(BF16)
+    return (high,) + split(member - high.astype(F32))
 
 
 def finish(masks, pack, sp, units, per, q_ref, ctx_ref, read_ref, maps, arrived, leaving,
@@ -166,28 +171,24 @@
     key_proj = mm(x, wk_ref[...]).astype(BF16).astype(F32)
     value_proj = mm(x, wv_ref[...]).astype(BF16).astype(F32)
 
-    source = iota((128, columns), 0)
+    spread = iota((128, columns), 0)
     target = iota((128, columns), 1) // HEAD
-    beta_pre = mm(gates, onehot(source == target))
-    decay_pre = mm(gates, onehot(source == target + heads))
-    source = iota((heads, columns), 0)
-    target = iota((heads, columns), 1) // HEAD
-    extra = lax.dot_general(extra_ref[0], onehot(source == target), (((0,), (0,)), ((), ())),
+    to_beta = onehot(spread == target)
+    to_decay = onehot(spread == target + heads)
+    place = iota((heads, 128), 0) + heads == iota((heads, 128), 1)
+    raw = gates.astype(F32)
+    softplus = jnp.maximum(raw, 0.0) + jnp.log1p(jnp.exp(-jnp.abs(raw)))
+    speed = jnp.dot(-jnp.exp(speed_ref[...]), jnp.where(place, 1.0, 0.0),
+                    precision=finest, preferred_element_type=F32)
+    extra = lax.dot_general(extra_ref[0], onehot(place), (((0,), (0,)), ((), ())),
                             preferred_element_type=F32)
-
-    beta = jax.nn.sigmoid(beta_pre)
-    softplus = jnp.maximum(decay_pre, 0.0) + jnp.log1p(jnp.exp(-jnp.abs(decay_pre)))
-    speed = jnp.dot(-jnp.exp(speed_ref[...]), jnp.where(source == target, 1.0, 0.0),
-                    precision=finest, preferred_element_type=F32)
     gamma = speed * softplus + extra
-    high = gamma.astype(BF16)
-    rest = gamma - high.astype(F32)
-    middle = rest.astype(BF16)
-    low = (rest - middle.astype(F32)).astype(BF16)
     r_idx = iota((rows, rows), 0)
     c_idx = iota((rows, rows), 1)
     running = onehot((r_idx >= c_idx) & (r_idx // HEAD == c_idx // HEAD))
-    cumul = mm(running, high) + mm(running, middle) + mm(running, low)
+    cumul = sum(mm(running, piece) for piece in thirds(gamma))
+    cumul = sum(mm(piece, to_decay) for piece in thirds(cumul))
+    beta = sum(mm(piece, to_beta) for piece in split(jax.nn.sigmoid(raw)))
 
     key = key_proj * jax.nn.sigmoid(key_proj)
     value = value_proj * jax.nn.sigmoid(value_proj)

time: 48.9 us -> 50.8 us (1.039)
  Pallas kernels: 45.4 us -> 47.3 us
    pallas_call x1, Pallas kernels: 45.4 us -> 47.3 us  [fused(): pl.pallas_call(functools.partial(kernel, per_seq, pack, sp), grid=(steps,...]
where the time goes in v4:
time: 50.8 us; the launch traced here: 50.7 us
  Pallas kernels  47.3 us (93%)
  local copies, waits for them, and re-layouts  2.72 us (5%)
  between operations  0.64 us (1%)
    pallas_call x1, Pallas kernels, fused(): pl.pallas_call(functools.partial(kernel, per_seq, pack, sp), grid=(steps,...  47.3 us
    unnamed x2, local copies, waits for them, and re-layouts  2.72 us

profile of v4, /device:TPU:0, one launch (start us, length us, event | category | flops | bytes accessed | tf_op | source)
XLA Modules:
  0.0 50.7 jit_solution(17869949641774941348)
XLA Ops:
  0.6 47.3 %shard_map.95 = (bf16[4,64,64]{2,1,0:T(8,128)(2,1)}, bf16[2,512]{1,0:T(2,128)(2,1)}) custom-call(bf16[1024,4096]{1,0:T(8,128)(2,1)} %bitcast.6, bf16[4096,512]{1,0:T(8,128)(2,1)} %wk_ref.1, bf16[4096,512]{1,0:T(8,128)(2,1)} %wv_ref.1, bf16[32,4096]{1,0:T(8,128)(2,1)} %bitcast.7, bf16[32,4096]{1,0:T(8,128)(2,1)} %bitcast.8, f32[1,8]{1,0:T(1,128)} %bitcast.11, ...), custom_call_target="tpu_custom_call" | custom-call | tf_op jit(solution)/shard_map/pallas_call | solution.py:363
  47.9 1.5 %copy.12 = bf16[2,8,16,64]{3,2,1,0:T(8,128)(2,1)} copy(bf16[2,8,16,64]{3,2,1,0:T(8,128)(2,1)} %bitcast.9) | data formatting | bytes 65536
  49.4 1.2 %copy.13 = bf16[2,512]{1,0:T(2,128)(2,1)} copy(bf16[2,512]{1,0:T(2,128)(2,1)} %get-tuple-element.9) | data formatting | bytes 4096
